TPU v7x, 32 devices: a whole 2x2x4 slice. The times are simulated.
32 devices in a mesh: sp: 8 (over z, y), tp: 4 (over x, core).
Axes of the slice: x: 2, y: 2, z: 4, core: 2. Of those that a mesh axis runs over, the one named last changes fastest.
Arguments:
- layer_source: bfloat16 [8192, 2048], P(('sp', 'tp')), may hold values from -6 to 6
- broad_probe_tensor: bfloat16 [8192, 512], P('sp', 'tp'), may hold values from -6 to 6
- broad_retention_preact: bfloat16 [8192, 512], P('sp', 'tp'), may hold values from -6 to 6
- broad_floor_margin: float32 [512], P('tp'), may hold values from 3.6621094e-05 to 0.12
- slim_probe_tensor: bfloat16 [8192, 256], P('sp', 'tp'), may hold values from -6 to 6
- slim_retention_preact: bfloat16 [8192, 256], P('sp', 'tp'), may hold values from -6 to 6
- slim_floor_margin: float32 [256], P('tp'), may hold values from 3.6621094e-05 to 0.12
- branch_content_tensor: bfloat16 [2, 8192, 512], P(None, 'sp', 'tp'), may hold values from -6 to 6
- emitted_switch_preact: bfloat16 [2, 8192, 512], P(None, 'sp', 'tp'), may hold values from -6 to 6
- extra_log_fades: float32 [2, 8192, 4], P(None, 'sp', 'tp'), may hold values from -1.4 to 0
- channel_norm_scale: float32 [128], replicated, may hold values from 0.1 to 1.9
- emission_projection: bfloat16 [2, 512, 2048], replicated, may hold values from -0.1875 to 0.1875
- mlp_norm_scale: float32 [2048], replicated, may hold values from 0.1 to 1.9
- switch_projection: bfloat16 [2048, 5632], P('sp', 'tp'), may hold values from -0.125 to 0.125
- expand_projection: bfloat16 [2048, 5632], P('sp', 'tp'), may hold values from -0.125 to 0.125
- shrink_projection: bfloat16 [5632, 2048], P('tp', 'sp'), may hold values from -0.078125 to 0.078125
Outputs:
- layer_out: bfloat16 [8192, 2048], P(('sp', 'tp'))
All inputs are finite; a program needn't handle non-finite values.
Results may differ from a plain program's by a relative error of at most 0.0095.
Values may be sent and summed in bfloat16 or wider, within the bound.
A program may use at most 192 MiB of HBM per device.

v0:
```python
import jax
import jax.numpy as jnp
from jax import lax
from jax.sharding import PartitionSpec as P

BRANCH_CHANNELS = 4
BLOCK = 64
EPSILON = 1e-06
EXACT_PRECISION = lax.Precision.HIGHEST


def entering(part, axis, combine, identity):
    place = lax.axis_index(axis)
    gathered = jax.tree.map(lambda a: lax.all_gather(a, axis), part)
    state = jax.tree.map(lambda a, e: jnp.zeros_like(a) + jnp.asarray(e, a.dtype), part, identity)

    def one(lap, state):
        return combine(
            state, jax.tree.map(lambda a: lax.dynamic_index_in_dim(a, lap, 0, False), gathered)
        )

    return lax.fori_loop(0, place, one, state)


def switched_token_entries(
    probe_array, retention_sigmoid, floor_margin, spike_rows, rows_of_values, count_heads
):
    length = probe_array.shape[0]
    key_width = probe_array.shape[1] // count_heads
    shaped = retention_sigmoid.astype(jnp.float32).reshape(length, count_heads, key_width)
    address_entries = floor_margin.reshape(count_heads, key_width) * jax.nn.sigmoid(-shaped)
    log_fade_amount = jnp.log1p(-address_entries) + spike_rows[:, :, None]
    probe_entries = jax.nn.silu(probe_array.astype(jnp.float32)).reshape(
        length, count_heads, key_width
    ) * key_width ** (-0.5)
    content_arrays = rows_of_values.astype(jnp.float32).reshape(length, count_heads, -1)
    return (probe_entries, address_entries, log_fade_amount, content_arrays)


def block_recurrence(probe_entries, address_entries, log_fade_amount, content_arrays, block_len):
    length, count_heads, key_width = probe_entries.shape
    value_width = content_arrays.shape[2]
    block_count = length // block_len

    def to_blocks(tensor):
        return jnp.moveaxis(
            tensor.reshape(block_count, block_len, count_heads, tensor.shape[2]), 2, 1
        )

    causal_mask = jnp.tril(jnp.ones((block_len, block_len), dtype=bool))[None, :, :, None]

    def advance(carried, inputs):
        state_stack, running = carried
        block_queries, key_block, block_values, decay_block = inputs
        prefix_decay = jnp.cumsum(decay_block, axis=1)
        state_contribution = jnp.einsum(
            "yga,yau->ygu",
            block_queries * jnp.exp(prefix_decay),
            state_stack,
            precision=EXACT_PRECISION,
        )
        relative = prefix_decay[:, :, None, :] - prefix_decay[:, None, :, :]
        decays = jnp.exp(jnp.where(causal_mask, relative, -jnp.inf))
        scores = jnp.einsum(
            "htk,hsk,htsk->hts", block_queries, key_block, decays, precision=EXACT_PRECISION
        )
        inside = jnp.einsum("hts,hsv->htv", scores, block_values, precision=EXACT_PRECISION)
        total_blocks = prefix_decay[:, -1, :]
        weighted_scores = key_block * jnp.exp(total_blocks[:, None, :] - prefix_decay)
        state_stack = jnp.exp(total_blocks)[:, :, None] * state_stack + jnp.einsum(
            "xpf,xpq->xfq", weighted_scores, block_values, precision=EXACT_PRECISION
        )
        reached_state = block_queries * jnp.exp(running[:, None, :] + prefix_decay)
        return ((state_stack, running + total_blocks), (state_contribution + inside, reached_state))

    initial = (
        jnp.zeros((count_heads, key_width, value_width), jnp.float32),
        jnp.zeros((count_heads, key_width), jnp.float32),
    )
    last_carry, (output_rows, reached_state) = lax.scan(
        advance,
        initial,
        (
            to_blocks(probe_entries),
            to_blocks(address_entries),
            to_blocks(content_arrays),
            to_blocks(log_fade_amount),
        ),
    )

    def from_blocks(tensor):
        return jnp.moveaxis(tensor, 1, 2).reshape(length, count_heads, tensor.shape[3])

    return (from_blocks(output_rows), from_blocks(reached_state), last_carry)


def head_norm(output_rows, channel_norm_scale, gate_rows):
    inverse = lax.rsqrt(jnp.mean(output_rows * output_rows, axis=2, keepdims=True) + EPSILON)
    normed = (output_rows * inverse * channel_norm_scale).reshape(output_rows.shape[0], -1)
    return (normed * jax.nn.silu(gate_rows.astype(jnp.float32))).astype(jnp.bfloat16)


def combine(earlier, later):
    wide_early, wide_state_early, narrow_early, narrow_state_early = earlier
    wide_late, wide_state_late, narrow_late, narrow_state_late = later
    return (
        wide_early + wide_late,
        jnp.exp(wide_late)[:, :, None] * wide_state_early + wide_state_late,
        narrow_early + narrow_late,
        jnp.exp(narrow_late)[:, :, None] * narrow_state_early + narrow_state_late,
    )


def local(
    layer_source,
    broad_probe_tensor,
    broad_retention_preact,
    broad_floor_margin,
    slim_probe_tensor,
    slim_retention_preact,
    slim_floor_margin,
    branch_content_tensor,
    emitted_switch_preact,
    extra_log_fades,
    channel_norm_scale,
    emission_projection,
    mlp_norm_scale,
    switch_projection,
    expand_projection,
    shrink_projection,
):
    tp_count = lax.axis_size("tp")
    count_heads = BRANCH_CHANNELS // tp_count
    row_count = layer_source.shape[0]
    groups = (
        (broad_probe_tensor, broad_retention_preact, broad_floor_margin),
        (slim_probe_tensor, slim_retention_preact, slim_floor_margin),
    )
    locals_out = []
    summaries = []
    for element_ordinal in range(2):
        probe_array, retention_sigmoid, floor_margin = groups[element_ordinal]
        probe_entries, address_entries, log_fade_amount, content_arrays = switched_token_entries(
            probe_array,
            retention_sigmoid,
            floor_margin,
            extra_log_fades[element_ordinal],
            branch_content_tensor[element_ordinal],
            count_heads,
        )
        output_rows, reached_state, last_carry = block_recurrence(
            probe_entries, address_entries, log_fade_amount, content_arrays, BLOCK
        )
        locals_out.append((output_rows, reached_state))
        summaries.append(last_carry)
    wide_state, wide_log = summaries[0]
    narrow_state, narrow_log = summaries[1]
    identity = (
        jnp.zeros_like(wide_log),
        jnp.zeros_like(wide_state),
        jnp.zeros_like(narrow_log),
        jnp.zeros_like(narrow_state),
    )
    carried = entering((wide_log, wide_state, narrow_log, narrow_state), "sp", combine, identity)
    incoming_state = (carried[1], carried[3])
    mixed_parts = []
    for element_ordinal in range(2):
        output_rows, reached_state = locals_out[element_ordinal]
        output_rows = output_rows + jnp.einsum(
            "qgj,gjw->qgw",
            reached_state,
            incoming_state[element_ordinal],
            precision=EXACT_PRECISION,
        )
        mixed_parts.append(
            head_norm(output_rows, channel_norm_scale, emitted_switch_preact[element_ordinal])
        )
    mixed = jnp.concatenate(mixed_parts, axis=1)
    group_width = branch_content_tensor.shape[2]
    model_width = emission_projection.shape[2]
    regrouped = lax.all_to_all(mixed, "tp", split_axis=0, concat_axis=1, tiled=True)
    shaped = regrouped.reshape(row_count, tp_count, 2, group_width)
    branch = jnp.einsum(
        "rtgc,gtcd->rd",
        shaped,
        emission_projection.reshape(2, tp_count, group_width, model_width),
        preferred_element_type=jnp.float32,
    )
    updated = layer_source.astype(jnp.float32) + branch
    inverse = lax.rsqrt(jnp.mean(updated * updated, axis=1, keepdims=True) + EPSILON)
    normed = (updated * inverse * mlp_norm_scale).astype(jnp.bfloat16)
    gate_full, up_full, down_full = (
        lax.all_gather(switch_projection, "sp", axis=0, tiled=True),
        lax.all_gather(expand_projection, "sp", axis=0, tiled=True),
        lax.all_gather(shrink_projection, "sp", axis=1, tiled=True),
    )
    row_piece = lax.all_gather(normed, "tp", axis=0, tiled=True)
    gate_part = jnp.dot(row_piece, gate_full, preferred_element_type=jnp.float32)
    up_part = jnp.dot(row_piece, up_full, preferred_element_type=jnp.float32)
    hidden = (jax.nn.silu(gate_part) * up_part).astype(jnp.bfloat16)
    ffn_sum = lax.psum_scatter(
        jnp.dot(hidden, down_full, preferred_element_type=jnp.float32).astype(jnp.bfloat16),
        "tp",
        scatter_dimension=0,
        tiled=True,
    ).astype(jnp.float32)
    return (updated + 0.5 * ffn_sum).astype(jnp.bfloat16)


def solution(mesh):
    placed = (
        P(("sp", "tp"), None),
        P("sp", "tp"),
        P("sp", "tp"),
        P("tp"),
        P("sp", "tp"),
        P("sp", "tp"),
        P("tp"),
        P(None, "sp", "tp"),
        P(None, "sp", "tp"),
        P(None, "sp", "tp"),
        P(),
        P(),
        P(),
        P("sp", "tp"),
        P("sp", "tp"),
        P("tp", "sp"),
    )
    return jax.shard_map(
        local, mesh=mesh, in_specs=placed, out_specs=P(("sp", "tp"), None), check_vma=False
    )
```

profile of v0, /device:TPU:0, one launch (start us, length us, event | category | flops | bytes accessed | tf_op | source)
XLA Modules:
  0.0 770.1 jit_solution(4900579919354530398)
XLA Ops:
  9.6 1.8 fusion.99
  13.4 179.5 %while.51 = (s32[]{:T(128)}, f32[1,64,128]{2,1,0:T(8,128)S(1)}, f32[1,64]{1,0:T(1,128)S(1)}, f32[16,1,64,128]{3,2,1,0:T(8,128)S(1)}, f32[16,1,64,64]{3,2,1,0:T(8...) while((s32[]{:T(128)}, f32[1,64,128]{2,1,0:T(8,128)S(1)}, ...), condition=%wide.region_5.6_spmd.clone, body=%wide.region_3.5_spmd.clone.sunk | while | flops 20504708 | bytes 4946317 | solution.py:80
  15.8 1.7 select_exponential_fusion.5
  17.5 3.3 copy.114
  27.0 1.7 select_exponential_fusion.5
  28.7 3.3 copy.114
  38.2 1.7 select_exponential_fusion.5
  39.9 3.3 copy.114
  49.4 1.7 select_exponential_fusion.5
  51.1 3.3 copy.114
  60.6 1.7 select_exponential_fusion.5
  62.4 3.3 copy.114
  71.9 1.7 select_exponential_fusion.5
  73.6 3.3 copy.114
  83.1 1.7 select_exponential_fusion.5
  84.8 3.3 copy.114
  94.3 1.7 select_exponential_fusion.5
  96.0 3.3 copy.114
  105.5 1.7 select_exponential_fusion.5
  107.2 3.3 copy.114
  116.7 1.7 select_exponential_fusion.5
  118.5 3.3 copy.114
  128.0 1.7 select_exponential_fusion.5
  129.7 3.3 copy.114
  139.2 1.7 select_exponential_fusion.5
  140.9 3.3 copy.114
  150.4 1.7 select_exponential_fusion.5
  152.1 3.3 copy.114
  161.6 1.7 select_exponential_fusion.5
  163.4 3.3 copy.114
  172.9 1.7 select_exponential_fusion.5
  174.6 3.3 copy.114
  184.1 1.7 select_exponential_fusion.5
  185.8 3.3 copy.114
  192.9 32.6 %all-gather.3 = f32[8,64,128]{2,1,0:T(8,128)S(1)} all-gather(f32[1,64,128]{2,1,0:T(8,128)S(1)} %get-tuple-element.189), channel_id=5, replica_groups=mesh['sp'=8,'tp'=4] {'sp'}, dimensions={0}, use_global_device_ids=true | all-gather | bytes 294912 | tf_op jit(solution)/shard_map/all_gather | solution.py:14
  225.5 20.6 %all-gather.5 = f32[8,1,64]{2,1,0:T(1,128)S(1)} all-gather(f32[1,1,64]{2,1,0:T(1,128)S(1)} %bitcast.343), channel_id=4, replica_groups=mesh['sp'=8,'tp'=4] {'sp'}, dimensions={0}, use_global_device_ids=true | all-gather | bytes 2304 | tf_op jit(solution)/shard_map/all_gather | solution.py:14
  248.1 2.1 divide_multiply_fusion
  250.3 64.7 %while.50 = (s32[]{:T(128)}, f32[1,128,128]{2,1,0:T(8,128)S(1)}, f32[1,128]{1,0:T(1,128)S(1)}, f32[16,1,64,128]{3,2,1,0:T(8,128)S(1)}, f32[16,1,64,128]{3,2,1,0:...) while((s32[]{:T(128)}, f32[1,128,128]{2,1,0:T(8,128)S(1)}, ...), condition=%wide.region_2.3_spmd.clone, body=%wide.region_0.2_spmd.clone.sunk | while | flops 34709760 | bytes 5176981 | solution.py:80
  251.9 1.7 fusion.165
  255.9 1.7 fusion.165
  260.0 1.7 fusion.165
  264.0 1.7 fusion.165
  268.1 1.7 fusion.165
  272.1 1.7 fusion.165
  276.1 1.7 fusion.165
  280.2 1.7 fusion.165
  284.2 1.7 fusion.165
  288.3 1.7 fusion.165
  292.3 1.7 fusion.165
  296.4 1.7 fusion.165
  300.4 1.7 fusion.165
  315.1 31.3 %all-gather.1 = f32[8,128,128]{2,1,0:T(8,128)S(1)} all-gather(f32[1,128,128]{2,1,0:T(8,128)S(1)} %get-tuple-element.187), channel_id=3, replica_groups=mesh['sp'=8,'tp'=4] {'sp'}, dimensions={0}, use_global_device_ids=true | all-gather | bytes 589824 | tf_op jit(solution)/shard_map/all_gather | solution.py:14
  346.3 16.3 %all-gather.4 = f32[8,1,128]{2,1,0:T(1,128)S(1)} all-gather(f32[1,1,128]{2,1,0:T(1,128)S(1)} %bitcast.342), channel_id=2, replica_groups=mesh['sp'=8,'tp'=4] {'sp'}, dimensions={0}, use_global_device_ids=true | all-gather | bytes 4608 | tf_op jit(solution)/shard_map/all_gather | solution.py:14
  363.1 1.8 multiply_reduce_fusion.1
  366.6 11.4 %all_to_all.13 = bf16[4,256,256]{2,1,0:T(8,128)(2,1)S(1)} all-to-all(bf16[4,256,256]{2,1,0:T(8,128)(2,1)S(1)} %pad_maximum_fusion), channel_id=1, replica_groups=mesh['sp'=8,'tp'=4] {'tp'}, dimensions={0} | all-to-all | bytes 1048576 | tf_op jit(solution)/shard_map/all_to_all | solution.py:181
  378.2 3.9 multiply_reduce_fusion
  385.6 31.5 %all-gather.11.cloned.1.call-done = bf16[1024,2048]{1,0:T(8,128)(2,1)} async-done(((bf16[256,2048]{1,0:T(8,128)(2,1)}), bf16[1024,2048]{1,0:T(8,128)(2,1)}) %all-gather.11.cloned.1.call-update) | async-done | bytes 4194320 | tf_op jit(solution)/shard_map/all_gather | solution.py:197
  417.1 94.5 %all-gather.13.cloned.1.call-done = bf16[2048,1408]{1,0:T(8,128)(2,1)} async-done(((bf16[256,1408]{1,0:T(8,128)(2,1)}), bf16[2048,1408]{1,0:T(8,128)(2,1)}) %all-gather.13.cloned.1.call-update) | async-done | bytes 5767184 | tf_op jit(solution)/shard_map/all_gather | solution.py:193
  511.6 11.6 %fusion.101 = f32[1024,1408]{1,0:T(8,128)} fusion(bf16[1024,2048]{1,0:T(8,128)(2,1)} %all-gather.11.cloned.1.call-done, bf16[2048,1408]{1,0:T(8,128)(2,1)} %all-gather.13.cloned.1.call-done), kind=kOutput, calls=%fused_computation.155 | convolution fusion | flops 5905580032 | bytes 15728640 | tf_op jit(solution)/shard_map/dot_general | solution.py:198
  523.3 81.1 %all-gather.15.cloned.1.call-done = bf16[2048,1408]{1,0:T(8,128)(2,1)} async-done(((bf16[256,1408]{1,0:T(8,128)(2,1)}), bf16[2048,1408]{1,0:T(8,128)(2,1)}) %all-gather.15.cloned.1.call-update) | async-done | bytes 5767184 | tf_op jit(solution)/shard_map/all_gather | solution.py:194
  604.3 93.2 %all-gather.17.cloned.1.call-done = bf16[1408,2048]{1,0:T(8,128)(2,1)} async-done(((bf16[1408,256]{1,0:T(8,128)(2,1)}), bf16[1408,2048]{1,0:T(8,128)(2,1)}) %all-gather.17.cloned.1.call-update) | async-done | bytes 5767184 | tf_op jit(solution)/shard_map/all_gather | solution.py:195
  697.6 20.6 %convolution_convert_fusion = bf16[1024,2048]{1,0:T(8,128)(2,1)} fusion(bf16[1408,2048]{1,0:T(8,128)(2,1)} %all-gather.17.cloned.1.call-done, f32[1024,1408]{1,0:T(8,128)} %fusion.101, bf16[1024,2048]{1,0:T(8,128)(2,1)} %all-gather.11.cloned.1.call-done, bf16[2048,1408]{1,0:T(8,128)(2,1)} %all-gather.15.cloned.1.call-done), kind=kOutput, calls=%fused_computation.101 | convolution fusion | flops 11821907968 | bytes 25690112 | tf_op jit(solution)/shard_map/dot_general | solution.py:202
  718.2 42.9 %reduce-scatter.2.cloned.1.call-done = bf16[256,2048]{1,0:T(8,128)(2,1)} async-done(((bf16[1024,2048]{1,0:T(8,128)(2,1)}), bf16[256,2048]{1,0:T(8,128)(2,1)}) %reduce-scatter.2.cloned.1.call-update) | async-done | bytes 1048592 | tf_op jit(solution)/shard_map/reduce_scatter | solution.py:201
  761.1 2.5 add_convert_fusion
  (471 shorter events, 151.6 us)
Async XLA Ops:
  6.5 5.7 copy-start.1
  6.5 410.6 %all-gather.11.cloned.1.call-start = ((), (), s32[]{:S(2)}) async-start(), calls=%async_computation.2 | async-start | bytes 5242880 | tf_op jit(solution)/shard_map/all_gather | solution.py:197
  362.7 2.9 copy-start.3
  363.1 2.9 copy-start
  378.2 3.9 copy-start.2
  383.3 128.3 %all-gather.13.cloned.1.call-start = ((), (), s32[]{:S(2)}) async-start(), calls=%async_computation.3 | async-start | bytes 6488064 | tf_op jit(solution)/shard_map/all_gather | solution.py:193
  384.1 220.3 %all-gather.15.cloned.1.call-start = ((), (), s32[]{:S(2)}) async-start(), calls=%async_computation.4 | async-start | bytes 6488064 | tf_op jit(solution)/shard_map/all_gather | solution.py:194
  384.8 312.8 %all-gather.17.cloned.1.call-start = ((), (), s32[]{:S(2)}) async-start(), calls=%async_computation.5 | async-start | bytes 6488064 | tf_op jit(solution)/shard_map/all_gather | solution.py:195
  385.4 375.7 %reduce-scatter.2.cloned.1.call-start = ((), (), s32[]{:S(2)}) async-start(), calls=%async_computation.6 | async-start | bytes 5242880 | tf_op jit(solution)/shard_map/reduce_scatter | solution.py:201
Sparse Core Ops, SparseCore 0:
  383.4 33.6 all-gather.10
  419.3 92.3 all-gather.12
  513.8 90.4 all-gather.14
  606.2 91.2 all-gather.16
  718.3 42.7 reduce-scatter.1
where the time goes:
time: 777 us; the launch traced here: 770 us
  waiting for transfers between devices  345 us (44%)
  other arithmetic  113 us (15%)
  blocking collectives  112 us (14%)
  matrix products  97.1 us (12%)
  local copies, waits for them, and re-layouts  86.6 us (11%)
  between operations  13.4 us (2%)
    all_gather x4, blocking collectives, entering(): gathered = jax.tree.map(lambda a: lax.all_gather(a, axis), part)  101 us
    all_gather x1, waiting for transfers between devices, local(): lax.all_gather(switch_projection, 'sp', axis=0, tiled=True)  94.5 us
    all_gather x1, waiting for transfers between devices, local(): lax.all_gather(shrink_projection, 'sp', axis=1, tiled=True)  93.2 us
    all_gather x1, waiting for transfers between devices, local(): lax.all_gather(expand_projection, 'sp', axis=0, tiled=True)  81.1 us
    while x16, local copies, waits for them, and re-layouts  53.2 us
    reduce_scatter x1, waiting for transfers between devices, local(): lax.psum_scatter(jnp.dot(hidden, down_full, preferred_element_type=jnp.fl...  42.9 us
    dot_general x32, other arithmetic, advance(): jnp.einsum('htk,hsk,htsk->hts', block_queries, key_block, decays, precisi...  38.5 us
    exp x32, other arithmetic, advance(): decays = jnp.exp(jnp.where(causal_mask, relative, -jnp.inf))  37.4 us
  transfers between devices with their start and end apart: 5, of which 5 were waited for; matrix products, arithmetic and copies ran while one was open for 2% of the time, Pallas kernels for 0%

commit v1 on v0

--- a/solution.py
+++ b/solution.py
@@ -192,7 +192,7 @@
     gate_full, up_full, down_full = (
         lax.all_gather(switch_projection, "sp", axis=0, tiled=True),
         lax.all_gather(expand_projection, "sp", axis=0, tiled=True),
-        lax.all_gather(shrink_projection, "sp", axis=1, tiled=True),
+        jnp.concatenate(lax.all_gather(shrink_projection, "sp"), axis=1),
     )
     row_piece = lax.all_gather(normed, "tp", axis=0, tiled=True)
     gate_part = jnp.dot(row_piece, gate_full, preferred_element_type=jnp.float32)

time: 777 us -> 705 us (0.907)
  waiting for transfers between devices: 345 us -> 244 us
  local copies, waits for them, and re-layouts: 86.6 us -> 108 us
  matrix products: 97.1 us -> 106 us
    all_gather x1, waiting for transfers between devices: 93.2 us -> 0.02 us  [local(): lax.all_gather(shrink_projection, 'sp')]
    another operation x69, local copies, waits for them, and re-layouts: 2.87 us -> 15.8 us
    dot_general x32, matrix products: 19.8 us -> 29.7 us  [advance(): jnp.einsum('hts,hsv->htv', scores, block_values, precision=EXACT_PRECISION)]
    reshape x0 -> x1, local copies, waits for them, and re-layouts: none -> 8.57 us  [local(): jnp.concatenate(lax.all_gather(shrink_projection, 'sp'), axis=1)]
    all_gather x1, waiting for transfers between devices: 31.5 us -> 23.4 us  [local(): row_piece = lax.all_gather(normed, 'tp', axis=0, tiled=True)]
  transfers between devices with their start and end apart: 5 -> 5, of which waited for: 5 -> 4; matrix products, arithmetic and copies ran while one was open for 2% -> 43% of each run, Pallas kernels for 0% -> 0%
where the time goes in v1:
time: 705 us; the launch traced here: 696 us
  waiting for transfers between devices  244 us (35%)
  blocking collectives  112 us (16%)
  other arithmetic  109 us (15%)
  local copies, waits for them, and re-layouts  108 us (15%)
  matrix products  106 us (15%)
  between operations  13.4 us (2%)
    all_gather x4, blocking collectives, entering(): gathered = jax.tree.map(lambda a: lax.all_gather(a, axis), part)  101 us
    all_gather x1, waiting for transfers between devices, local(): lax.all_gather(switch_projection, 'sp', axis=0, tiled=True)  94.5 us
    all_gather x1, waiting for transfers between devices, local(): lax.all_gather(expand_projection, 'sp', axis=0, tiled=True)  80.9 us
    while x16, local copies, waits for them, and re-layouts  53.2 us
    reduce_scatter x1, waiting for transfers between devices, local(): lax.psum_scatter(jnp.dot(hidden, down_full, preferred_element_type=jnp.fl...  42.9 us
    dot_general x32, other arithmetic, advance(): jnp.einsum('htk,hsk,htsk->hts', block_queries, key_block, decays, precisi...  38.8 us
    exp x32, other arithmetic, advance(): decays = jnp.exp(jnp.where(causal_mask, relative, -jnp.inf))  36.9 us
    dot_general x32, matrix products, advance(): jnp.einsum('hts,hsv->htv', scores, block_values, precision=EXACT_PRECISION)  29.7 us
  transfers between devices with their start and end apart: 5, of which 4 were waited for; matrix products, arithmetic and copies ran while one was open for 43% of the time, Pallas kernels for 0%

profile of v1, /device:TPU:0, one launch (start us, length us, event | category | flops | bytes accessed | tf_op | source)
XLA Modules:
  0.0 696.3 jit_solution(15834204758576608434)
XLA Ops:
  14.8 65.0 %while.50 = (s32[]{:T(128)}, f32[1,128,128]{2,1,0:T(8,128)S(1)}, f32[1,128]{1,0:T(1,128)S(1)}, f32[16,1,64,128]{3,2,1,0:T(8,128)S(1)}, f32[16,1,64,128]{3,2,1,0:...) while((s32[]{:T(128)}, f32[1,128,128]{2,1,0:T(8,128)S(1)}, ...), condition=%wide.region_2.3_spmd.clone, body=%wide.region_0.2_spmd.clone.sunk | while | flops 34709760 | bytes 5176981 | solution.py:80
  16.3 1.7 fusion.165
  20.4 1.7 fusion.165
  24.5 1.7 fusion.165
  28.5 1.7 fusion.165
  32.6 1.7 fusion.165
  36.6 1.7 fusion.165
  40.7 1.7 fusion.165
  44.8 1.7 fusion.165
  48.8 1.7 fusion.165
  52.9 1.7 fusion.165
  57.0 1.7 fusion.165
  61.0 1.7 fusion.165
  65.1 1.7 fusion.165
  69.2 1.7 fusion.165
  73.2 1.7 fusion.165
  77.3 1.7 fusion.165
  80.6 200.7 %while.51 = (s32[]{:T(128)}, f32[1,64,128]{2,1,0:T(8,128)S(1)}, f32[1,64]{1,0:T(1,128)S(1)}, f32[16,1,64,128]{3,2,1,0:T(8,128)}, f32[16,1,64,64]{3,2,1,0:T(8,128...) while((s32[]{:T(128)}, f32[1,64,128]{2,1,0:T(8,128)S(1)}, ...), condition=%wide.region_5.6_spmd.clone, body=%wide.region_3.5_spmd.clone.sunk | while | flops 20504708 | bytes 4913037 | solution.py:80
  83.0 1.7 select_exponential_fusion.5
  84.7 3.3 copy.117
  95.5 1.7 select_exponential_fusion.5
  97.2 3.3 copy.117
  108.1 1.7 select_exponential_fusion.5
  109.8 3.3 copy.117
  120.6 1.7 select_exponential_fusion.5
  122.3 3.3 copy.117
  133.2 1.7 select_exponential_fusion.5
  134.9 3.3 copy.117
  145.7 1.7 select_exponential_fusion.5
  147.4 3.3 copy.117
  158.3 1.7 select_exponential_fusion.5
  160.0 3.3 copy.117
  170.8 1.7 select_exponential_fusion.5
  172.5 3.3 copy.117
  183.4 1.7 select_exponential_fusion.5
  185.0 3.3 copy.117
  195.9 1.7 select_exponential_fusion.5
  197.6 3.3 copy.117
  208.4 1.7 select_exponential_fusion.5
  210.1 3.3 copy.117
  221.0 1.7 select_exponential_fusion.5
  222.7 3.3 copy.117
  233.5 1.7 select_exponential_fusion.5
  235.2 3.3 copy.117
  246.1 1.7 select_exponential_fusion.5
  247.8 3.3 copy.117
  258.6 1.7 select_exponential_fusion.5
  260.3 3.3 copy.117
  271.2 1.7 select_exponential_fusion.5
  272.9 3.3 copy.117
  282.8 22.4 %all-gather.6 = f32[8,1,64]{2,1,0:T(1,128)S(1)} all-gather(f32[1,1,64]{2,1,0:T(1,128)S(1)} %bitcast.351), channel_id=4, replica_groups=mesh['sp'=8,'tp'=4] {'sp'}, dimensions={0}, use_global_device_ids=true | all-gather | bytes 2304 | tf_op jit(solution)/shard_map/all_gather | solution.py:14
  305.2 16.3 %all-gather.5 = f32[8,1,128]{2,1,0:T(1,128)S(1)} all-gather(f32[1,1,128]{2,1,0:T(1,128)S(1)} %bitcast.352), channel_id=2, replica_groups=mesh['sp'=8,'tp'=4] {'sp'}, dimensions={0}, use_global_device_ids=true | all-gather | bytes 4608 | tf_op jit(solution)/shard_map/all_gather | solution.py:14
  321.5 31.0 %all-gather.3 = f32[8,64,128]{2,1,0:T(8,128)S(1)} all-gather(f32[1,64,128]{2,1,0:T(8,128)S(1)} %get-tuple-element.189), channel_id=5, replica_groups=mesh['sp'=8,'tp'=4] {'sp'}, dimensions={0}, use_global_device_ids=true | all-gather | bytes 294912 | tf_op jit(solution)/shard_map/all_gather | solution.py:14
  352.5 31.4 %all-gather.1 = f32[8,128,128]{2,1,0:T(8,128)S(1)} all-gather(f32[1,128,128]{2,1,0:T(8,128)S(1)} %get-tuple-element.187), channel_id=3, replica_groups=mesh['sp'=8,'tp'=4] {'sp'}, dimensions={0}, use_global_device_ids=true | all-gather | bytes 589824 | tf_op jit(solution)/shard_map/all_gather | solution.py:14
  386.4 11.4 %all_to_all.13 = bf16[4,256,256]{2,1,0:T(8,128)(2,1)S(1)} all-to-all(bf16[4,256,256]{2,1,0:T(8,128)(2,1)S(1)} %pad_maximum_fusion), channel_id=1, replica_groups=mesh['sp'=8,'tp'=4] {'tp'}, dimensions={0} | all-to-all | bytes 1048576 | tf_op jit(solution)/shard_map/all_to_all | solution.py:181
  398.0 3.9 multiply_reduce_fusion
  404.7 8.6 %copy.87 = bf16[1408,8,256]{0,2,1:T(8,128)(2,1)} copy(bf16[1408,8,256]{2,0,1:T(8,128)(2,1)} %bitcast.329) | data formatting | bytes 11534336 | tf_op jit(solution)/shard_map/reshape | solution.py:195
  413.2 23.4 %all-gather.12.cloned.1.call-done = bf16[1024,2048]{1,0:T(8,128)(2,1)} async-done(((bf16[256,2048]{1,0:T(8,128)(2,1)}), bf16[1024,2048]{1,0:T(8,128)(2,1)}) %all-gather.12.cloned.1.call-update) | async-done | bytes 4194320 | tf_op jit(solution)/shard_map/all_gather | solution.py:197
  436.7 94.5 %all-gather.14.cloned.1.call-done = bf16[2048,1408]{1,0:T(8,128)(2,1)} async-done(((bf16[256,1408]{1,0:T(8,128)(2,1)}), bf16[2048,1408]{1,0:T(8,128)(2,1)}) %all-gather.14.cloned.1.call-update) | async-done | bytes 5767184 | tf_op jit(solution)/shard_map/all_gather | solution.py:193
  531.2 11.7 %fusion.101 = f32[1024,1408]{1,0:T(8,128)} fusion(bf16[1024,2048]{1,0:T(8,128)(2,1)} %all-gather.12.cloned.1.call-done, bf16[2048,1408]{1,0:T(8,128)(2,1)} %all-gather.14.cloned.1.call-done), kind=kOutput, calls=%fused_computation.155 | convolution fusion | flops 5905580032 | bytes 15728640 | tf_op jit(solution)/shard_map/dot_general | solution.py:198
  542.9 80.9 %all-gather.16.cloned.1.call-done = bf16[2048,1408]{1,0:T(8,128)(2,1)} async-done(((bf16[256,1408]{1,0:T(8,128)(2,1)}), bf16[2048,1408]{1,0:T(8,128)(2,1)}) %all-gather.16.cloned.1.call-update) | async-done | bytes 5767184 | tf_op jit(solution)/shard_map/all_gather | solution.py:194
  623.7 20.6 %convolution_convert_fusion = bf16[1024,2048]{1,0:T(8,128)(2,1)} fusion(bf16[1408,2048]{0,1:T(8,128)(2,1)} %bitcast.330, f32[1024,1408]{1,0:T(8,128)} %fusion.101, bf16[1024,2048]{1,0:T(8,128)(2,1)} %all-gather.12.cloned.1.call-done, bf16[2048,1408]{1,0:T(8,128)(2,1)} %all-gather.16.cloned.1.call-done), kind=kOutput, calls=%fused_computation.101 | convolution fusion | flops 11821907968 | bytes 25690112 | tf_op jit(solution)/shard_map/dot_general | solution.py:202
  644.4 42.9 %reduce-scatter.2.cloned.1.call-done = bf16[256,2048]{1,0:T(8,128)(2,1)} async-done(((bf16[1024,2048]{1,0:T(8,128)(2,1)}), bf16[256,2048]{1,0:T(8,128)(2,1)}) %reduce-scatter.2.cloned.1.call-update) | async-done | bytes 1048592 | tf_op jit(solution)/shard_map/reduce_scatter | solution.py:201
  687.3 2.5 add_convert_fusion
  (482 shorter events, 171.4 us)
Async XLA Ops:
  6.5 4.8 copy-start.1
  6.5 5.7 copy-start.5
  6.5 398.1 %all-gather.18.cloned.1.call-start = ((), (), s32[]{:S(2)}) async-start(), calls=%async_computation.6 | async-start | bytes 6488064 | tf_op jit(solution)/shard_map/all_gather | solution.py:195
  7.3 429.4 %all-gather.12.cloned.1.call-start = ((), (), s32[]{:S(2)}) async-start(), calls=%async_computation.2 | async-start | bytes 5242880 | tf_op jit(solution)/shard_map/all_gather | solution.py:197
  8.1 5.3 copy-start.3
  10.3 3.3 copy-start.4
  10.3 3.3 copy-start.7
  282.8 101.1 %copy-start = (f32[16,1,64,64]{3,2,1,0:T(8,128)S(1)}, f32[16,1,64,64]{3,2,1,0:T(8,128)}, u32[]{:S(2)}) copy-start(f32[16,1,64,64]{3,2,1,0:T(8,128)} %get-tuple-element.194) | copy-start | bytes 786436
  352.5 32.8 %copy-start.8 = (f32[128]{0:T(128)S(1)}, f32[128]{0:T(128)}, u32[]{:S(2)}) copy-start(f32[128]{0:T(128)} %param.32) | copy-start | bytes 1540
  384.6 1.3 copy-start.2
  398.0 3.9 copy-start.6
  403.1 128.1 %all-gather.14.cloned.1.call-start = ((), (), s32[]{:S(2)}) async-start(), calls=%async_computation.3 | async-start | bytes 6488064 | tf_op jit(solution)/shard_map/all_gather | solution.py:193
  403.8 219.9 %all-gather.16.cloned.1.call-start = ((), (), s32[]{:S(2)}) async-start(), calls=%async_computation.4 | async-start | bytes 6488064 | tf_op jit(solution)/shard_map/all_gather | solution.py:194
  404.4 282.9 %reduce-scatter.2.cloned.1.call-start = ((), (), s32[]{:S(2)}) async-start(), calls=%async_computation.5 | async-start | bytes 5242880 | tf_op jit(solution)/shard_map/reduce_scatter | solution.py:201
Sparse Core Ops, SparseCore 0:
  9.5 95.2 all-gather.17
  403.2 33.4 all-gather.11
  438.8 92.3 all-gather.13
  533.2 90.4 all-gather.15
  644.5 42.7 reduce-scatter.1
